TPU v7x, 32 devices: a whole 2x2x4 slice. The times are simulated.
32 devices in a mesh: sp: 8 (over z, y), dp: 4 (over x, core).
Axes of the slice: x: 2, y: 2, z: 4, core: 2. Of those that a mesh axis runs over, the one named last changes fastest.
Arguments:
- tokens: bfloat16 [4, 1024, 2048], P('dp', 'sp'), may hold values from -6 to 6
- cotangent: bfloat16 [4, 1024, 2048], P('dp', 'sp'), may hold values from -6 to 6
- value_weight: bfloat16 [2048, 2048], P(('sp', 'dp')), may hold values from -0.125 to 0.125
- query_heads: bfloat16 [4, 1024, 16, 128], P('dp', None, 'sp'), may hold values from -8 to 8
- key_heads: bfloat16 [4, 1024, 16, 128], P('dp', None, 'sp'), may hold values from -8 to 8
- lambdas: float32 [16], P('sp'), may hold values from 0.3 to 0.8
Outputs:
- grad_query: bfloat16 [4, 1024, 16, 128], P('dp', None, 'sp')
- grad_key: bfloat16 [4, 1024, 16, 128], P('dp', None, 'sp')
- grad_tokens: bfloat16 [4, 1024, 2048], P('dp', 'sp')
- grad_value_weight: float32 [2048, 2048], P(('sp', 'dp'))
- grad_lambda: float32 [16], P('sp')
All inputs are finite; a program needn't handle non-finite values.
Results may differ from a plain program's by a relative error of at most 0.0095.
Values may be sent and summed in bfloat16 or wider, within the bound.
A program may use at most 192 MiB of HBM per device.

v0:
```python
import jax
import jax.numpy as jnp
from jax import lax
from jax.sharding import PartitionSpec as P

QBLOCK = 256


EPS = 1e-06
NEGATIVE = -1e30


def head_backward(queries, keys_in, values_in, cotangent, lambdas, block_rows):
    seq_length = queries.shape[0]
    head_count = queries.shape[1]
    head_width = queries.shape[3]
    scaling = head_width ** (-0.5)
    blocks_count = seq_length // block_rows
    lambda_col = lambdas[:, None, None]
    grad_key_sum = jnp.zeros(keys_in.shape, jnp.float32)
    grad_value_sum = jnp.zeros(values_in.shape, jnp.float32)
    grad_lambda_sum = jnp.zeros((head_count,), jnp.float32)
    query_blocks = []
    for block_index in range(blocks_count):
        offset = block_index * block_rows
        reach = offset + block_rows
        query_block = queries[offset:reach]
        cotan_block = cotangent[offset:reach].astype(jnp.float32)
        keys_seen = keys_in[:reach]
        values_seen = values_in[:reach]
        scores = (
            jnp.einsum(
                "qhcd,khcd->hcqk", query_block, keys_seen, preferred_element_type=jnp.float32
            )
            * scaling
        )
        rows_pos = offset + jnp.arange(block_rows, dtype=jnp.int32)
        allowed = rows_pos[:, None] >= jnp.arange(reach, dtype=jnp.int32)[None, :]
        scores = jnp.where(allowed, scores, NEGATIVE)
        highest = jnp.max(scores, axis=-1, keepdims=True)
        exponent = jnp.exp(scores - highest)
        softmaxes = exponent / jnp.sum(exponent, axis=-1, keepdims=True)
        weights = (softmaxes[:, 0] - lambda_col * softmaxes[:, 1]).astype(jnp.bfloat16)
        mixed_out = jnp.einsum(
            "hqk,khd->qhd", weights, values_seen, preferred_element_type=jnp.float32
        )
        inverse = lax.rsqrt(jnp.mean(mixed_out * mixed_out, axis=-1, keepdims=True) + EPS)
        normed = mixed_out * inverse
        grad_mixed = (
            inverse
            * (cotan_block - normed * jnp.mean(cotan_block * normed, axis=-1, keepdims=True))
        ).astype(jnp.bfloat16)
        grad_weights = jnp.einsum(
            "qhd,khd->hqk", grad_mixed, values_seen, preferred_element_type=jnp.float32
        )
        value_part = jnp.einsum(
            "hqk,qhd->khd", weights, grad_mixed, preferred_element_type=jnp.float32
        )
        grad_value_sum = grad_value_sum.at[:reach].add(value_part)
        grad_lambda_sum = grad_lambda_sum - jnp.sum(grad_weights * softmaxes[:, 1], axis=(1, 2))
        first_grad = softmaxes[:, 0] * (
            grad_weights - jnp.sum(grad_weights * softmaxes[:, 0], axis=-1, keepdims=True)
        )
        second_grad = (
            -lambda_col
            * softmaxes[:, 1]
            * (grad_weights - jnp.sum(grad_weights * softmaxes[:, 1], axis=-1, keepdims=True))
        )
        grad_scores = (jnp.stack([first_grad, second_grad], axis=1) * scaling).astype(jnp.bfloat16)
        query_blocks.append(
            jnp.einsum(
                "hcqk,khcd->qhcd", grad_scores, keys_seen, preferred_element_type=jnp.float32
            ).astype(jnp.bfloat16)
        )
        key_part = jnp.einsum(
            "hcqk,qhcd->khcd", grad_scores, query_block, preferred_element_type=jnp.float32
        )
        grad_key_sum = grad_key_sum.at[:reach].add(key_part)
    grad_query = jnp.concatenate(query_blocks, axis=0)
    return (
        grad_query,
        grad_key_sum.astype(jnp.bfloat16),
        grad_value_sum.astype(jnp.bfloat16),
        grad_lambda_sum,
    )


def body(tokens, cotangent, value_weight, query_heads, key_heads, lambdas):
    local_tokens = tokens[0]
    row_count = value_weight.shape[0]
    value_rows = jnp.dot(
        local_tokens,
        lax.all_gather(value_weight, ("sp", "dp"), axis=0, tiled=True),
        preferred_element_type=jnp.float32,
    )
    value_tokens = value_rows.astype(jnp.bfloat16)[None]
    cotan_heads, value_heads = (
        lax.all_to_all(cotangent, "sp", split_axis=2, concat_axis=1, tiled=True),
        lax.all_to_all(value_tokens, "sp", split_axis=2, concat_axis=1, tiled=True),
    )
    seq_length = cotan_heads.shape[1]
    head_count = query_heads.shape[2]
    head_width = query_heads.shape[3] // 2
    queries = query_heads[0].reshape(seq_length, head_count, 2, head_width)
    keys_in = key_heads[0].reshape(seq_length, head_count, 2, head_width)
    values_in = value_heads[0].reshape(seq_length, head_count, 2 * head_width)
    cotan_in = cotan_heads[0].reshape(seq_length, head_count, 2 * head_width)
    grad_query, grad_key, grad_value, grad_lambda = head_backward(
        queries, keys_in, values_in, cotan_in, lambdas, QBLOCK
    )
    lambda_grad = lax.psum(grad_lambda, "dp")
    grad_value_local = grad_value.reshape(seq_length, head_count * 2 * head_width)
    grad_value_tokens = lax.all_to_all(
        grad_value_local[None], "sp", split_axis=1, concat_axis=2, tiled=True
    )[0]
    grad_rows = lax.dot_general(
        grad_value_tokens,
        lax.all_gather(value_weight, ("sp", "dp"), axis=0, tiled=True),
        (((1,), (1,)), ((), ())),
        preferred_element_type=jnp.float32,
    )
    grad_tokens = grad_rows.astype(jnp.bfloat16)[None]
    all_tokens = lax.all_gather(tokens, "sp", axis=1, tiled=True)[0]
    sp_count = lax.axis_size("sp")
    dp_count = lax.axis_size("dp")
    token_blocks = all_tokens.reshape(seq_length, sp_count, dp_count, row_count)
    group_rows = sp_count * row_count
    term = jnp.einsum(
        "lsdb,lf->dsbf", token_blocks, grad_value_local, preferred_element_type=jnp.float32
    )
    by_batch = lax.psum_scatter(
        term.reshape(group_rows * lax.axis_size("dp"), grad_value_local.shape[1]).astype(
            jnp.bfloat16
        ),
        "dp",
        scatter_dimension=0,
        tiled=True,
    ).astype(jnp.float32)
    grad_weight = lax.all_to_all(
        by_batch.astype(jnp.bfloat16), "sp", split_axis=0, concat_axis=1, tiled=True
    ).astype(by_batch.dtype)
    grad_query_out = grad_query.reshape(1, seq_length, head_count, 2 * head_width)
    grad_key_out = grad_key.reshape(1, seq_length, head_count, 2 * head_width)
    return (grad_query_out, grad_key_out, grad_tokens, grad_weight, lambda_grad)


def solution(mesh):
    placed = (
        P("dp", "sp", None),
        P("dp", "sp", None),
        P(("sp", "dp"), None),
        P("dp", None, "sp", None),
        P("dp", None, "sp", None),
        P("sp"),
    )
    return jax.shard_map(
        body,
        mesh=mesh,
        in_specs=placed,
        out_specs=(
            P("dp", None, "sp", None),
            P("dp", None, "sp", None),
            P("dp", "sp", None),
            P(("sp", "dp"), None),
            P("sp"),
        ),
        check_vma=False,
    )
```

profile of v0, /device:TPU:0, one launch (start us, length us, event | category | flops | bytes accessed | tf_op | source)
XLA Modules:
  0.0 284.3 jit_solution(9939884770805880808)
XLA Ops:
  10.8 11.5 %reduce.16 = bf16[2048,128]{1,0:T(8,128)(2,1)S(1)} reduce(bf16[2048,1,128]{2,1,0:T(2,128)(2,1)S(1)} %bitcast.324, bf16[]{:T(256)} %broadcast.337), dimensions={1}, to_apply=%bitcast.242.reduce_sub_computation | reduce | bytes 1048578
  23.2 7.4 %all-to-all-start.1 = ((bf16[8,2,16384]{2,1,0:T(2,128)(2,1)}), bf16[8,2,16384]{2,1,0:T(2,128)(2,1)}, u32[]{:S(2)}, u32[]{:S(2)}) async-start(bf16[8,2,16384]{2,1,0:T(2,128)(2,1)} %reshape.398), calls=%async_computation.1 | async-start | bytes 1048576 | tf_op jit(solution)/shard_map/all_to_all | solution.py:98
  45.6 4.7 %fusion.155 = (f32[2,2,256]{2,1,0:T(2,128)S(1)}, f32[2,2,256,1024]{3,2,1,0:T(8,128)}) fusion(pred[256,1024]{1,0:T(8,128)(4,1)} %iota_compare_fusion, bf16[256,2,2,64]{0,3,2,1:T(8,128)(2,1)S(1)} %bitcast.335, bf16[1024,2,2,64]{0,3,2,1:T(8,128)(2,1)} %bitcast.343), kind=kOutput, calls=%fused_computation.202 | convolution fusion | flops 138413056 | bytes 5115904 | tf_op jit(solution)/shard_map/sub | solution.py:41
  50.3 4.8 %broadcast_divide_fusion = f32[2,2,256,1024]{3,2,1,0:T(8,128)} fusion(f32[2,2,256,1024]{3,2,1,0:T(8,128)} %get-tuple-element.153, f32[2,2,256]{2,1,0:T(2,128)S(1)} %get-tuple-element.152), kind=kLoop, calls=%fused_computation.38 | loop fusion | flops 1048576 | bytes 8392704 | tf_op jit(solution)/shard_map/div | solution.py:42
  58.9 34.5 %all-gather.3.cloned.1.call-done = bf16[2048,2048]{1,0:T(8,128)(2,1)} async-done(((bf16[64,2048]{1,0:T(8,128)(2,1)}), bf16[2048,2048]{1,0:T(8,128)(2,1)}) %all-gather.3.cloned.1.call-update) | async-done | bytes 8388624 | tf_op jit(solution)/shard_map/all_gather | solution.py:93
  93.4 5.6 %fusion.18 = bf16[1,128,2048]{2,1,0:T(8,128)(2,1)} fusion(bf16[2048,2048]{1,0:T(8,128)(2,1)} %all-gather.3.cloned.1.call-done, bf16[1,128,2048]{2,1,0:T(8,128)(2,1)} %param.26), kind=kOutput, calls=%fused_computation.26 | convolution fusion | flops 1074003968 | bytes 9437184 | tf_op jit(solution)/shard_map/dot_general | solution.py:91
  99.0 3.6 %copy.202 = bf16[1,128,2048]{1,0,2:T(2,128)(2,1)} copy(bf16[1,128,2048]{2,1,0:T(8,128)(2,1)} %fusion.18) | data formatting | bytes 1048576 | tf_op jit(solution)/shard_map/broadcast_in_dim | solution.py:96
  102.6 13.9 %reduce.17 = bf16[2048,128]{1,0:T(8,128)(2,1)} reduce(bf16[2048,1,128]{2,1,0:T(2,128)(2,1)} %bitcast.326, bf16[]{:T(256)} %broadcast.337), dimensions={1}, to_apply=%bitcast.244.reduce_sub_computation | reduce | bytes 1048578
  118.4 4.1 %all-to-all-start = ((bf16[8,2,16384]{2,1,0:T(2,128)(2,1)}), bf16[8,2,16384]{2,1,0:T(2,128)(2,1)}, u32[]{:S(2)}, u32[]{:S(2)}) async-start(bf16[8,2,16384]{2,1,0:T(2,128)(2,1)} %reshape.400), calls=%async_computation | async-start | bytes 1048576 | tf_op jit(solution)/shard_map/all_to_all | solution.py:99
  127.6 3.7 %reshape.399 = bf16[2048,1,128]{2,1,0:T(2,128)(2,1)} reshape(bf16[8,2,16384]{2,1,0:T(2,128)(2,1)} %all-to-all-done.1) | data formatting | bytes 1048576
  140.9 6.0 %all-to-all-done = bf16[8,2,16384]{2,1,0:T(2,128)(2,1)} async-done(((bf16[8,2,16384]{2,1,0:T(2,128)(2,1)}), bf16[8,2,16384]{2,1,0:T(2,128)(2,1)}, u32[]{:S(2)}, u32[]{:S(2)}) %all-to-all-start) | async-done | bytes 524320 | tf_op jit(solution)/shard_map/all_to_all | solution.py:99
  146.9 3.5 %reshape.401 = bf16[2048,1,128]{2,1,0:T(2,128)(2,1)} reshape(bf16[8,2,16384]{2,1,0:T(2,128)(2,1)} %all-to-all-done) | data formatting | bytes 1048576
  181.9 3.1 %fusion.54 = f32[2,1,256,512]{3,2,0,1:T(8,128)} fusion(f32[2,2,256,512]{3,2,1,0:T(8,128)} %copy-done.1, bf16[256,2,128]{0,2,1:T(8,128)(2,1)S(1)} %multiply_convert_fusion.2, bf16[512,2,128]{0,2,1:T(8,128)(2,1)S(1)} %slice.331), kind=kOutput, calls=%fused_computation.71 | convolution fusion | flops 135005184 | bytes 3932160 | tf_op jit(solution)/shard_map/sub | solution.py:62
  185.0 3.0 %fusion.57 = f32[2,1,256,512]{3,2,0,1:T(8,128)} fusion(f32[2,2,256,512]{3,2,1,0:T(8,128)} %copy-done.1, f32[2]{0:T(128)S(1)} %neg.3, bf16[256,2,128]{0,2,1:T(8,128)(2,1)S(1)} %multiply_convert_fusion.2, bf16[512,2,128]{0,2,1:T(8,128)(2,1)S(1)} %slice.331), kind=kOutput, calls=%fused_computation.74 | convolution fusion | flops 135267328 | bytes 3932672 | tf_op jit(solution)/shard_map/sub | solution.py:67
  196.7 3.7 %fusion = f32[2,256,1024]{2,1,0:T(8,128)} fusion(f32[2,2,256,1024]{3,2,1,0:T(8,128)} %broadcast_divide_fusion, bf16[256,2,128]{0,2,1:T(8,128)(2,1)S(1)} %multiply_convert_fusion, bf16[1024,2,128]{0,2,1:T(8,128)(2,1)} %reshape_squeeze.12), kind=kOutput, calls=%fused_computation | convolution fusion | flops 134743552 | bytes 4849664 | tf_op jit(solution)/shard_map/sub | solution.py:67
  200.4 4.1 %fusion.13 = f32[256,2048]{0,1:S(1)} fusion(bf16[1024,256]{0,1:T(8,128)(2,1)} %bitcast.332, bf16[1,1024,2048]{2,1,0:T(8,128)(2,1)} %all-gather.5.cloned.1.call-done), kind=kOutput, calls=%fused_computation.14 | convolution fusion | flops 1073741824 | bytes 6815744
  205.8 3.7 %copy.243 = bf16[1,1024,256]{2,0,1:T(2,128)(2,1)} copy(bf16[1,1024,256]{1,2,0:T(8,128)(2,1)} %bitcast.333) | data formatting | bytes 1048576 | tf_op jit(solution)/shard_map/broadcast_in_dim;reshape | solution.py:114
  209.5 5.6 %reduce.18 = bf16[1024,256]{1,0:T(8,128)(2,1)} reduce(bf16[1024,1,256]{2,1,0:T(2,128)(2,1)} %bitcast.325, bf16[]{:T(256)} %broadcast.337), dimensions={1}, to_apply=%bitcast.246.reduce_sub_computation | reduce | bytes 1048578
  217.1 4.8 %fusion.150 = (f32[2]{0:T(128)S(1)}, f32[2,1,256,1024]{3,2,0,1:T(8,128)}) fusion(f32[2,2,256,1024]{3,2,1,0:T(8,128)} %broadcast_divide_fusion, f32[2,256,1024]{2,1,0:T(8,128)} %fusion, f32[2]{0:T(128)S(1)} %neg.3, bf16[256,2,128]{0,2,1:T(8,128)(2,1)S(1)} %multiply_convert_fusion, bf16[1024,2,128]{0,2,1:T(8,128)(2,1)} %reshape_squeeze.12), kind=kOutput, calls=%fused_computation.198 | convolution fusion | flops 136839168 | bytes 6946832 | tf_op jit(solution)/shard_map/qhd,khd->hqk/dot_general | solution.py:53
  222.4 7.6 %all-to-all-start.2 = ((bf16[8,2,16384]{2,1,0:T(2,128)(2,1)}), bf16[8,2,16384]{2,1,0:T(2,128)(2,1)}, u32[]{:S(2)}, u32[]{:S(2)}) async-start(bf16[8,2,16384]{2,1,0:T(2,128)(2,1)} %reshape.402), calls=%async_computation.2 | async-start | bytes 1048576 | tf_op jit(solution)/shard_map/all_to_all | solution.py:113
  230.0 6.3 %psum.7 = f32[2]{0:T(128)} all-reduce(f32[2]{0:T(128)} %subtract_subtract_fusion), channel_id=1, replica_groups=mesh['sp'=8,'dp'=4] {'dp'}, use_global_device_ids=true, to_apply=%region_29.30 | all-reduce | flops 2 | bytes 16 | tf_op jit(solution)/shard_map/psum | solution.py:111
  241.8 4.5 %multiply_bitcast_fusion.1 = f32[2,1,256,1024]{3,2,0,1:T(8,128)} fusion(f32[2,2,256,1024]{3,2,1,0:T(8,128)} %broadcast_divide_fusion, bf16[256,2,128]{0,2,1:T(8,128)(2,1)S(1)} %multiply_convert_fusion, bf16[1024,2,128]{0,2,1:T(8,128)(2,1)S(1)} %copy-done.4), kind=kOutput, calls=%fused_computation.34 | convolution fusion | flops 270009856 | bytes 7602176 | tf_op jit(solution)/shard_map/sub | solution.py:62
  261.7 6.4 %all-to-all-start.3 = ((bf16[8,64,256]{2,1,0:T(8,128)(2,1)}), bf16[8,64,256]{2,1,0:T(8,128)(2,1)S(1)}, u32[]{:S(2)}, u32[]{:S(2)}) async-start(bf16[8,64,256]{2,1,0:T(8,128)(2,1)} %bitcast.352), calls=%async_computation.4 | async-start | bytes 524288 | tf_op jit(solution)/shard_map/all_to_all | solution.py:139
  268.1 7.1 %fusion.19 = bf16[1,128,2048]{2,1,0:T(8,128)(2,1)} fusion(bf16[128,2048]{0,1:T(8,128)(2,1)S(1)} %bitcast.328, bf16[2048,2048]{1,0:T(8,128)(2,1)} %all-gather.3.cloned.1.call-done), kind=kOutput, calls=%fused_computation.27 | convolution fusion | flops 1074003968 | bytes 9437184 | tf_op jit(solution)/shard_map/dot_general | solution.py:116
  (238 shorter events, 106.4 us)
Async XLA Ops:
  7.2 86.2 %all-gather.3.cloned.1.call-start = ((), (), s32[]{:S(2)}) async-start(), calls=%async_computation.5 | async-start | bytes 8650752 | tf_op jit(solution)/shard_map/all_gather | solution.py:93
  22.3 9.8 %copy-start.26 = (bf16[1,1024,2,128]{3,2,1,0:T(2,128)(2,1)S(1)}, bf16[1,1024,2,128]{3,2,1,0:T(2,128)(2,1)}, u32[]{:S(2)}) copy-start(bf16[1,1024,2,128]{3,2,1,0:T(2,128)(2,1)} %param.30) | copy-start | bytes 1572868
  23.2 10.1 %slice-start = ((bf16[1,1024,2,128]{3,2,1,0:T(2,128)(2,1)}), bf16[1,256,2,128]{3,2,1,0:T(2,128)(2,1)S(1)}, s32[]{:S(2)}) async-start(bf16[1,1024,2,128]{3,2,1,0:T(2,128)(2,1)} %param.30), calls=%async_computation.8 | async-start | bytes 262144 | tf_op jit(solution)/shard_map/slice | solution.py:29
  23.2 95.2 %all-to-all-start.1 = ((bf16[8,2,16384]{2,1,0:T(2,128)(2,1)}), bf16[8,2,16384]{2,1,0:T(2,128)(2,1)}, u32[]{:S(2)}, u32[]{:S(2)}) async-start(bf16[8,2,16384]{2,1,0:T(2,128)(2,1)} %reshape.398), calls=%async_computation.1 | async-start | bytes 1048576 | tf_op jit(solution)/shard_map/all_to_all | solution.py:98
  30.7 4.6 %slice-start.1 = ((bf16[1,1024,2,128]{3,2,1,0:T(2,128)(2,1)}), bf16[1,512,2,128]{3,2,1,0:T(2,128)(2,1)S(1)}, s32[]{:S(2)}) async-start(bf16[1,1024,2,128]{3,2,1,0:T(2,128)(2,1)} %param.30), calls=%async_computation.9 | async-start | bytes 524288 | tf_op jit(solution)/shard_map/slice | solution.py:29
  30.7 169.7 %all-gather.5.cloned.1.call-start = ((), (), s32[]{:S(2)}) async-start(), calls=%async_computation.6 | async-start | bytes 4718592 | tf_op jit(solution)/shard_map/all_gather | solution.py:123
  31.4 4.0 %slice-start.2 = ((bf16[1,1024,2,128]{3,2,1,0:T(2,128)(2,1)}), bf16[1,768,2,128]{3,2,1,0:T(2,128)(2,1)S(1)}, s32[]{:S(2)}) async-start(bf16[1,1024,2,128]{3,2,1,0:T(2,128)(2,1)} %param.30), calls=%async_computation.10 | async-start | bytes 786432 | tf_op jit(solution)/shard_map/slice | solution.py:29
  33.5 21.6 %copy-start.44 = (bf16[1,256,2,128]{1,3,2,0:T(8,128)(2,1)}, bf16[1,256,2,128]{1,3,2,0:T(8,128)(2,1)S(1)}, u32[]{:S(2)}) copy-start(bf16[1,256,2,128]{1,3,2,0:T(8,128)(2,1)S(1)} %copy.199) | copy-start | bytes 393220
  35.9 4.6 %copy-start.47 = (bf16[1,768,2,128]{1,3,2,0:T(8,128)(2,1)}, bf16[1,768,2,128]{1,3,2,0:T(8,128)(2,1)S(1)}, u32[]{:S(2)}) copy-start(bf16[1,768,2,128]{1,3,2,0:T(8,128)(2,1)S(1)} %copy.220) | copy-start | bytes 1179652
  36.4 18.7 %copy-start.41 = (bf16[1,256,2,128]{1,3,2,0:T(8,128)(2,1)}, bf16[1,256,2,128]{1,3,2,0:T(8,128)(2,1)S(1)}, u32[]{:S(2)}) copy-start(bf16[1,256,2,128]{1,3,2,0:T(8,128)(2,1)S(1)} %copy.198) | copy-start | bytes 393220
  36.7 8.9 %copy-start.35 = (bf16[1,256,2,128]{1,3,2,0:T(8,128)(2,1)}, bf16[1,256,2,128]{1,3,2,0:T(8,128)(2,1)S(1)}, u32[]{:S(2)}) copy-start(bf16[1,256,2,128]{1,3,2,0:T(8,128)(2,1)S(1)} %copy.229) | copy-start | bytes 393220
  50.3 4.8 %copy-start.53 = (pred[256,256]{0,1:T(8,128)(4,1)S(1)}, pred[256,256]{0,1:T(8,128)(4,1)}, u32[]{:S(2)}) copy-start(pred[256,256]{0,1:T(8,128)(4,1)} %iota_compare_fusion.3) | copy-start | bytes 196612
  118.4 28.5 %all-to-all-start = ((bf16[8,2,16384]{2,1,0:T(2,128)(2,1)}), bf16[8,2,16384]{2,1,0:T(2,128)(2,1)}, u32[]{:S(2)}, u32[]{:S(2)}) async-start(bf16[8,2,16384]{2,1,0:T(2,128)(2,1)} %reshape.400), calls=%async_computation | async-start | bytes 1048576 | tf_op jit(solution)/shard_map/all_to_all | solution.py:99
  122.6 139.1 %reduce-scatter.2.cloned.1.call-start = ((), (), s32[]{:S(2)}) async-start(), calls=%async_computation.7 | async-start | bytes 1310720 | tf_op jit(solution)/shard_map/reduce_scatter | solution.py:131
  172.1 3.9 %copy-start.16 = (bf16[256,2,128]{0,2,1:T(8,128)(2,1)S(1)}, bf16[256,2,128]{0,2,1:T(8,128)(2,1)}, u32[]{:S(2)}) copy-start(bf16[256,2,128]{0,2,1:T(8,128)(2,1)} %multiply_convert_fusion.3) | copy-start | bytes 393220
  172.1 3.9 %copy-start.27 = (bf16[2,256,256]{1,2,0:T(8,128)(2,1)S(1)}, bf16[2,256,256]{1,2,0:T(8,128)(2,1)}, u32[]{:S(2)}) copy-start(bf16[2,256,256]{1,2,0:T(8,128)(2,1)} %subtract_convert_fusion.3) | copy-start | bytes 786436
  217.1 4.8 %copy-start.55 = (f32[2]{0:T(128)S(1)}, f32[2]{0:T(128)}, u32[]{:S(2)}) copy-start(f32[2]{0:T(128)} %fusion.123) | copy-start | bytes 28
  217.1 4.8 %copy-start.56 = (f32[2]{0:T(128)S(1)}, f32[2]{0:T(128)}, u32[]{:S(2)}) copy-start(f32[2]{0:T(128)} %fusion.134) | copy-start | bytes 28
  217.1 19.2 %copy-start.50 = (bf16[1,512,2,128]{1,3,2,0:T(8,128)(2,1)S(1)}, bf16[1,512,2,128]{1,3,2,0:T(8,128)(2,1)}, u32[]{:S(2)}) copy-start(bf16[1,512,2,128]{1,3,2,0:T(8,128)(2,1)} %copy-done.49) | copy-start | bytes 786436
  222.4 36.7 %all-to-all-start.2 = ((bf16[8,2,16384]{2,1,0:T(2,128)(2,1)}), bf16[8,2,16384]{2,1,0:T(2,128)(2,1)}, u32[]{:S(2)}, u32[]{:S(2)}) async-start(bf16[8,2,16384]{2,1,0:T(2,128)(2,1)} %reshape.402), calls=%async_computation.2 | async-start | bytes 1048576 | tf_op jit(solution)/shard_map/all_to_all | solution.py:113
  241.8 4.5 %copy-start.12 = (f32[2,1,256,1024]{3,2,0,1:T(8,128)S(1)}, f32[2,1,256,1024]{3,2,0,1:T(8,128)}, u32[]{:S(2)}) copy-start(f32[2,1,256,1024]{3,2,0,1:T(8,128)} %get-tuple-element.143) | copy-start | bytes 6291460
  241.8 4.5 %copy-start.43 = (bf16[1,1024,2,128]{1,3,2,0:T(8,128)(2,1)S(1)}, bf16[1,1024,2,128]{1,3,2,0:T(8,128)(2,1)}, u32[]{:S(2)}) copy-start(bf16[1,1024,2,128]{1,3,2,0:T(8,128)(2,1)} %copy.230) | copy-start | bytes 1572868
  249.6 4.1 %copy-start.40 = (bf16[1,256,2,128]{1,3,2,0:T(8,128)(2,1)S(1)}, bf16[1,256,2,128]{1,3,2,0:T(8,128)(2,1)}, u32[]{:S(2)}) copy-start(bf16[1,256,2,128]{1,3,2,0:T(8,128)(2,1)} %copy-done.39) | copy-start | bytes 393220
  261.7 14.9 %all-to-all-start.3 = ((bf16[8,64,256]{2,1,0:T(8,128)(2,1)}), bf16[8,64,256]{2,1,0:T(8,128)(2,1)S(1)}, u32[]{:S(2)}, u32[]{:S(2)}) async-start(bf16[8,64,256]{2,1,0:T(8,128)(2,1)} %bitcast.352), calls=%async_computation.4 | async-start | bytes 524288 | tf_op jit(solution)/shard_map/all_to_all | solution.py:139
  (43 other events, 89.9 us)
Sparse Core Ops, SparseCore 0:
  10.8 82.4 all-gather.2
  95.5 76.3 all-gather.4
  205.9 27.6 reduce-scatter.1
where the time goes:
time: 290 us; the launch traced here: 284 us
  matrix products  70.5 us (24%)
  local copies, waits for them, and re-layouts  63.4 us (22%)
  other arithmetic  60.3 us (21%)
  waiting for transfers between devices  43 us (15%)
  starting transfers between devices  26 us (9%)
  between operations  14.8 us (5%)
  blocking collectives  6.28 us (2%)
    all_gather x1, waiting for transfers between devices, body(): lax.all_gather(value_weight, ('sp', 'dp'), axis=0, tiled=True)  34.5 us
    unnamed x128, local copies, waits for them, and re-layouts  31.3 us
    unnamed x4, other arithmetic  31 us
    sub x4, matrix products, head_backward(): exponent = jnp.exp(scores - highest)  10.1 us
    sub x3, matrix products, head_backward(): grad_weights - jnp.sum(grad_weights * softmaxes[:, 0], axis=-1, keepdims=...  10 us
    div x4, other arithmetic, head_backward(): softmaxes = exponent / jnp.sum(exponent, axis=-1, keepdims=True)  9.48 us
    sub x3, matrix products, head_backward(): grad_weights - jnp.sum(grad_weights * softmaxes[:, 1], axis=-1, keepdims=...  9.28 us
    dot_general x4, matrix products, head_backward(): jnp.einsum('qhd,khd->hqk', grad_mixed, values_seen, preferred_element_typ...  8.35 us
  transfers between devices with their start and end apart: 7, of which 3 were waited for; matrix products, arithmetic and copies ran while one was open for 64% of the time, Pallas kernels for 0%

commit v1 on v0

v1 whole, which is shorter than its diff:
```python
import functools

import jax
import jax.numpy as jnp
from jax import lax
from jax.experimental import pallas as pl
from jax.experimental.pallas import tpu as pltpu
from jax.sharding import PartitionSpec as P

QBLOCK = 256
EPS = 1e-06
NEGATIVE = -1e30
CHUNKS = 2
F32 = jnp.float32
BF16 = jnp.bfloat16


def dot_nn(a, b):
    return jnp.dot(a, b, preferred_element_type=F32)


def dot_nt(a, b):
    return lax.dot_general(a, b, (((1,), (1,)), ((), ())), preferred_element_type=F32)


def attention_kernel(
    lam_ref, q_ref, k_ref, v_ref, g_ref, gq_ref, gk_ref, gv_ref, gl_ref, gk_acc, gv_acc
):
    length, width = q_ref.shape
    half = width // 2
    block = min(QBLOCK, length)
    scaling = half ** (-0.5)
    lam = lam_ref[pl.program_id(0)]
    lanes = lax.broadcasted_iota(jnp.int32, (length, width), 1)
    first_half = lanes < half
    q_all = q_ref[...].astype(F32) * scaling
    k_all = k_ref[...].astype(F32) * scaling
    q_halves = [
        jnp.where(first_half, q_all, 0.0).astype(BF16),
        jnp.where(first_half, 0.0, q_all).astype(BF16),
    ]
    kt_halves = [
        jnp.where(first_half, k_all, 0.0).T.astype(BF16),
        jnp.where(first_half, 0.0, k_all).T.astype(BF16),
    ]
    vt = v_ref[...].astype(F32).T.astype(BF16)
    gt = g_ref[...].astype(F32).T
    keep = lax.broadcasted_iota(jnp.int32, (block, block), 0) <= lax.broadcasted_iota(
        jnp.int32, (block, block), 1
    )
    lambda_total = jnp.zeros((1, block), F32)
    for index in range(length // block):
        off = index * block
        reach = off + block
        pieces = ([(0, off)] if off else []) + [(off, reach)]
        probs = []
        for c in range(2):
            qc = q_halves[c][off:reach]
            scores = [dot_nt(k_ref[lo:hi], qc) for lo, hi in pieces]
            scores[-1] = jnp.where(keep, scores[-1], NEGATIVE)
            top = functools.reduce(
                jnp.maximum, [jnp.max(s, axis=0, keepdims=True) for s in scores]
            )
            exps = [jnp.exp(s - top) for s in scores]
            total = sum(jnp.sum(e, axis=0, keepdims=True) for e in exps)
            inv = 1.0 / total
            probs.append([e * inv for e in exps])
        weights = [(p1 - lam * p2).astype(BF16) for p1, p2 in zip(*probs)]
        out_t = sum(dot_nn(vt[:, lo:hi], w) for (lo, hi), w in zip(pieces, weights))
        cot = gt[:, off:reach]
        inverse = lax.rsqrt(jnp.mean(out_t * out_t, axis=0, keepdims=True) + EPS)
        normed = out_t * inverse
        grad_out = (
            inverse * (cot - normed * jnp.mean(cot * normed, axis=0, keepdims=True))
        ).astype(BF16)
        grad_w = [dot_nn(v_ref[lo:hi], grad_out) for lo, hi in pieces]
        sums = [
            sum(jnp.sum(d * p, axis=0, keepdims=True) for d, p in zip(grad_w, probs[c]))
            for c in range(2)
        ]
        lambda_total = lambda_total - sums[1]
        first = [(p * (d - sums[0])).astype(BF16) for d, p in zip(grad_w, probs[0])]
        second = [(-lam * p * (d - sums[1])).astype(BF16) for d, p in zip(grad_w, probs[1])]
        gq_t = sum(
            dot_nn(kt_halves[0][:, lo:hi], a) + dot_nn(kt_halves[1][:, lo:hi], b)
            for (lo, hi), a, b in zip(pieces, first, second)
        )
        gq_ref[off:reach, :] = gq_t.T.astype(BF16)
        for (lo, hi), w, a, b in zip(pieces, weights, first, second):
            gv = dot_nt(w, grad_out)
            gk = dot_nn(a, q_halves[0][off:reach]) + dot_nn(b, q_halves[1][off:reach])
            if lo == off:
                gv_acc[lo:hi, :] = gv
                gk_acc[lo:hi, :] = gk
            else:
                gv_acc[lo:hi, :] += gv
                gk_acc[lo:hi, :] += gk
    gk_ref[...] = gk_acc[...].astype(BF16)
    gv_ref[...] = gv_acc[...].astype(BF16)
    gl_ref[...] = jnp.broadcast_to(jnp.sum(lambda_total, axis=1, keepdims=True), gl_ref.shape[1:])[
        None
    ]


def attention(lambdas, queries, keys, values, cotangent, width):
    length, features = queries.shape
    heads = features // width
    column = pl.BlockSpec((length, width), lambda h: (0, h))
    shape = jax.ShapeDtypeStruct((length, features), BF16)
    return pl.pallas_call(
        attention_kernel,
        grid=(heads,),
        in_specs=[pl.BlockSpec(memory_space=pltpu.SMEM)] + [column] * 4,
        out_specs=[column] * 3 + [pl.BlockSpec((1, 8, 128), lambda h: (h, 0, 0))],
        out_shape=[shape] * 3 + [jax.ShapeDtypeStruct((heads, 8, 128), F32)],
        scratch_shapes=[pltpu.VMEM((length, width), F32)] * 2,
        compiler_params=pltpu.CompilerParams(vmem_limit_bytes=48 * 1024 * 1024),
        cost_estimate=pl.CostEstimate(
            flops=12 * length * length * width * heads,
            bytes_accessed=14 * length * features,
            transcendentals=length * length * heads,
        ),
        name="attention",
    )(lambdas, queries, keys, values, cotangent)


def remote(src, dst, send, recv, sp, dp):
    return pltpu.make_async_remote_copy(
        src_ref=src,
        dst_ref=dst,
        send_sem=send,
        recv_sem=recv,
        device_id=(sp, dp),
        device_id_type=pl.DeviceIdType.MESH,
    )


def ring_place(sp, n):
    odd = sp % 2
    return (1 - odd) * (sp // 2) + odd * (n - 1 - sp // 2)


def ring_member(place, n):
    late = place // (n // 2)
    return (1 - late) * (2 * place) + late * (2 * (n - 1 - place) + 1)


def greet(peers):
    barrier = pltpu.get_barrier_semaphore()
    for sp, dp in peers:
        pl.semaphore_signal(
            barrier, inc=1, device_id=(sp, dp), device_id_type=pl.DeviceIdType.MESH
        )
    pl.semaphore_wait(barrier, len(peers))


def gather_kernel(
    n,
    m,
    tok_ref,
    cot_ref,
    w_ref,
    all_ref,
    coth_ref,
    wc_ref,
    local_sem,
    ring_send,
    ring_recv,
    a_send,
    a_recv,
    x_send,
    x_recv,
    c_send,
    c_recv,
):
    me = lax.axis_index("sp")
    my_dp = lax.axis_index("dp")
    rows = tok_ref.shape[0]
    feats = coth_ref.shape[2]
    part = rows // (2 * CHUNKS)
    place = ring_place(me, n)
    sides = [
        ring_member((place + 1) % n, n),
        ring_member((place + n - 1) % n, n),
    ]
    core = my_dp + 1 - 2 * (my_dp % 2)
    sp_peers = [(me + k) % n for k in range(1, n)]
    x_peers = [(my_dp + 2 * k) % m for k in range(1, m // 2)]
    greet(
        [(s, my_dp) for s in sp_peers] + [(me, d) for d in x_peers] + [(me, core)]
    )

    def columns(ref, s):
        return ref.at[:, pl.ds(pl.multiple_of(s * feats, feats), feats)]

    w_copies = [
        remote(columns(w_ref, s), wc_ref.at[me, my_dp], a_send.at[0, k], a_recv.at[0, k], s, my_dp)
        for k, s in enumerate(sp_peers)
    ]
    for copy in w_copies:
        copy.start()

    def ring(step, side, chunk):
        origin = (place + n - step) % n if side == 0 else (place + step) % n
        block = ring_member(origin, n)
        span = pl.ds((side * CHUNKS + chunk) * part, part)
        src = tok_ref.at[span] if step == 0 else all_ref.at[block, span]
        return remote(
            src,
            all_ref.at[block, span],
            ring_send.at[step, side, chunk],
            ring_recv.at[step, side, chunk],
            sides[side],
            my_dp,
        )

    order = [(side, chunk) for chunk in range(CHUNKS) for side in range(2)]
    hops = {}
    for side, chunk in order:
        hops[0, side, chunk] = ring(0, side, chunk)
        hops[0, side, chunk].start()
    locals_ = [
        pltpu.make_async_copy(tok_ref, all_ref.at[me], local_sem.at[0]),
        pltpu.make_async_copy(columns(cot_ref, me), coth_ref.at[me], local_sem.at[1]),
        pltpu.make_async_copy(columns(w_ref, me), wc_ref.at[me, my_dp], local_sem.at[2]),
    ]
    for copy in locals_:
        copy.start()
    cot_copies = [
        remote(columns(cot_ref, s), coth_ref.at[me], a_send.at[1, k], a_recv.at[1, k], s, my_dp)
        for k, s in enumerate(sp_peers)
    ]
    for copy in cot_copies:
        copy.start()
    locals_[2].wait()
    for copy in w_copies:
        copy.wait_recv()
    x_copies = [
        remote(wc_ref.at[:, my_dp], wc_ref.at[:, my_dp], x_send.at[k], x_recv.at[k], me, d)
        for k, d in enumerate(x_peers)
    ]
    for copy in x_copies:
        copy.start()
    c_copies = [remote(wc_ref.at[:, my_dp], wc_ref.at[:, my_dp], c_send.at[0], c_recv.at[0], me, core)]
    c_copies[0].start()
    for step in range(1, n - 1):
        for side, chunk in order:
            hops[step - 1, side, chunk].wait_recv()
            hops[step, side, chunk] = ring(step, side, chunk)
            hops[step, side, chunk].start()
        if step == n // 2:
            for k in range(1, m // 2):
                origin = (my_dp + m - 2 * k) % m
                x_copies[k - 1].wait_recv()
                copy = remote(
                    wc_ref.at[:, origin], wc_ref.at[:, origin], c_send.at[k], c_recv.at[k], me, core
                )
                copy.start()
                c_copies.append(copy)
    for side, chunk in order:
        hops[n - 2, side, chunk].wait_recv()
    for copy in cot_copies + c_copies:
        copy.wait_recv()
    for copy in list(hops.values()) + w_copies + cot_copies + x_copies + c_copies:
        copy.wait_send()
    locals_[0].wait()
    locals_[1].wait()


def gather(tokens, cotangent, weight, n, m):
    rows, depth = tokens.shape
    feats = weight.shape[1] // n
    vmem = pl.BlockSpec(memory_space=pltpu.VMEM)
    dma = pltpu.SemaphoreType.DMA
    return pl.pallas_call(
        functools.partial(gather_kernel, n, m),
        out_shape=[
            jax.ShapeDtypeStruct((n, rows, depth), BF16),
            jax.ShapeDtypeStruct((n, rows, feats), BF16),
            jax.ShapeDtypeStruct((n, m, weight.shape[0], feats), BF16),
        ],
        in_specs=[vmem] * 3,
        out_specs=[vmem] * 3,
        scratch_shapes=[
            dma((3,)),
            dma((n - 1, 2, CHUNKS)),
            dma((n - 1, 2, CHUNKS)),
            dma((2, n - 1)),
            dma((2, n - 1)),
            dma((max(m // 2 - 1, 1),)),
            dma((max(m // 2 - 1, 1),)),
            dma((m // 2,)),
            dma((m // 2,)),
        ],
        compiler_params=pltpu.CompilerParams(
            collective_id=0, has_side_effects=True, vmem_limit_bytes=40 * 1024 * 1024
        ),
        cost_estimate=pl.CostEstimate(
            flops=40_000_000_000, bytes_accessed=20_000_000, transcendentals=0
        ),
        name="gather",
    )(tokens, cotangent, weight)


def scatter_kernel(
    n, m, dv_ref, t_ref, gl_ref, dvt_ref, gw_ref, glo_ref, rbuf, sbuf, fbuf, lbuf,
    local_sem, v_send, v_recv, t_send, t_recv, l_send, l_recv, f_send, f_recv,
):
    me = lax.axis_index("sp")
    my_dp = lax.axis_index("dp")
    rows = dvt_ref.shape[0]
    feats = dv_ref.shape[1]
    sp_peers = [(me + k) % n for k in range(1, n)]
    dp_peers = [(my_dp + k) % m for k in range(1, m)]
    greet([(s, my_dp) for s in sp_peers] + [(me, d) for d in dp_peers])

    def tokens_of(s):
        return dv_ref.at[pl.ds(pl.multiple_of(s * rows, rows), rows)]

    mine = dvt_ref.at[:, pl.ds(pl.multiple_of(me * feats, feats), feats)]
    t_copies = [
        remote(t_ref.at[d], rbuf.at[k], t_send.at[k], t_recv.at[k], me, d)
        for k, d in enumerate(dp_peers)
    ]
    l_copies = [
        remote(gl_ref, lbuf.at[k], l_send.at[k], l_recv.at[k], me, d)
        for k, d in enumerate(dp_peers)
    ]
    v_copies = [
        remote(tokens_of(s), mine, v_send.at[k], v_recv.at[k], s, my_dp)
        for k, s in enumerate(sp_peers)
    ]
    for copy in l_copies + t_copies + v_copies:
        copy.start()
    own = pltpu.make_async_copy(tokens_of(me), mine, local_sem.at[0])
    own.start()
    for copy in t_copies:
        copy.wait_recv()
    total = t_ref[my_dp].astype(F32)
    for k in range(m - 1):
        total = total + rbuf[k].astype(F32)
    sbuf[...] = total.astype(BF16)
    f_copies = [
        remote(sbuf.at[s], fbuf.at[me], f_send.at[k], f_recv.at[k], s, my_dp)
        for k, s in enumerate(sp_peers)
    ]
    for copy in f_copies:
        copy.start()
    own_f = pltpu.make_async_copy(sbuf.at[me], fbuf.at[me], local_sem.at[1])
    own_f.start()
    for copy in l_copies:
        copy.wait_recv()
    lam = gl_ref[...]
    for k in range(m - 1):
        lam = lam + lbuf[k]
    glo_ref[...] = lam
    own_f.wait()
    for copy in f_copies:
        copy.wait_recv()
    for s in range(n):
        gw_ref[:, s * feats : (s + 1) * feats] = fbuf[s].astype(F32)
    own.wait()
    for copy in v_copies:
        copy.wait_recv()
    for copy in l_copies + t_copies + v_copies + f_copies:
        copy.wait_send()


def scatter(grad_value, term, grad_lambda, n, m):
    length, feats = grad_value.shape
    row_count = term.shape[2]
    vmem = pl.BlockSpec(memory_space=pltpu.VMEM)
    dma = pltpu.SemaphoreType.DMA
    return pl.pallas_call(
        functools.partial(scatter_kernel, n, m),
        out_shape=[
            jax.ShapeDtypeStruct((length // n, n * feats), BF16),
            jax.ShapeDtypeStruct((row_count, n * feats), F32),
            jax.ShapeDtypeStruct(grad_lambda.shape, F32),
        ],
        in_specs=[vmem] * 3,
        out_specs=[vmem] * 3,
        scratch_shapes=[
            pltpu.VMEM((m - 1,) + term.shape[1:], BF16),
            pltpu.VMEM(term.shape[1:], BF16),
            pltpu.VMEM(term.shape[1:], BF16),
            pltpu.VMEM((m - 1,) + grad_lambda.shape, F32),
            dma((2,)),
            dma((n - 1,)),
            dma((n - 1,)),
            dma((m - 1,)),
            dma((m - 1,)),
            dma((m - 1,)),
            dma((m - 1,)),
            dma((n - 1,)),
            dma((n - 1,)),
        ],
        compiler_params=pltpu.CompilerParams(
            collective_id=1, has_side_effects=True, vmem_limit_bytes=40 * 1024 * 1024
        ),
        name="scatter",
    )(grad_value, term, grad_lambda)


def body(n, m, tokens, cotangent, value_weight, query_heads, key_heads, lambdas):
    row_count, feature_count = value_weight.shape
    all_weight = lax.all_gather(value_weight, ("sp", "dp"), axis=0, tiled=True)
    all_tokens, cotan_heads, weight_cols = gather(tokens[0], cotangent[0], value_weight, n, m)
    feats = feature_count // n
    depth = n * m * row_count
    length = all_tokens.shape[0] * all_tokens.shape[1]
    head_count, width = query_heads.shape[2], query_heads.shape[3]
    flat_tokens = all_tokens.reshape(length, depth)
    values = jnp.dot(
        flat_tokens, weight_cols.reshape(depth, feats), preferred_element_type=F32
    ).astype(BF16)
    grad_query, grad_key, grad_value, grad_lambda = attention(
        lambdas,
        query_heads.reshape(length, feats),
        key_heads.reshape(length, feats),
        values,
        cotan_heads.reshape(length, feats),
        width,
    )
    term = lax.dot_general(
        flat_tokens, grad_value, (((0,), (0,)), ((), ())), preferred_element_type=F32
    ).astype(BF16)
    term = term.reshape(n, m, row_count, feats).transpose(1, 0, 2, 3)
    grad_value_tokens, grad_weight, lambda_sum = scatter(grad_value, term, grad_lambda, n, m)
    grad_tokens = dot_nt(grad_value_tokens, all_weight).astype(BF16)[None]
    return (
        grad_query.reshape(1, length, head_count, width),
        grad_key.reshape(1, length, head_count, width),
        grad_tokens,
        grad_weight,
        lambda_sum[:, 0, 0],
    )


def solution(mesh):
    placed = (
        P("dp", "sp", None),
        P("dp", "sp", None),
        P(("sp", "dp"), None),
        P("dp", None, "sp", None),
        P("dp", None, "sp", None),
        P("sp"),
    )
    return jax.shard_map(
        functools.partial(body, mesh.shape["sp"], mesh.shape["dp"]),
        mesh=mesh,
        in_specs=placed,
        out_specs=(
            P("dp", None, "sp", None),
            P("dp", None, "sp", None),
            P("dp", "sp", None),
            P(("sp", "dp"), None),
            P("sp"),
        ),
        check_vma=False,
    )
```

time: 290 us -> 171 us (0.59); the launches traced: 284 us -> 169 us
  Pallas kernels: 0 us -> 134 us
  other arithmetic: 60.3 us -> 0 us
  matrix products: 70.5 us -> 11.8 us
  local copies, waits for them, and re-layouts: 63.4 us -> 8.43 us
  waiting for transfers between devices: 43 us -> 0.68 us
  starting transfers between devices: 26 us -> 0.04 us
  blocking collectives: 6.28 us -> 0 us
    pallas_call x0 -> x3, Pallas kernels: none -> 134 us  [the longest x1 102 us: gather(): pl.pallas_call(functools.partial(gather_kernel, n, m), out_shape=[jax.Sha...]
    all_gather x2 -> x1, waiting for transfers between devices: 34.5 us -> 0.01 us  [body(): all_weight = lax.all_gather(value_weight, ('sp', 'dp'), axis=0, tiled=True)]
    unnamed x4 -> x0, other arithmetic: 31 us -> none
    sub x10 -> x0, matrix products: 29.4 us -> none  [the longest x4 10.1 us: head_backward(): exponent = jnp.exp(scores - highest)]
    unnamed x128 -> x11, local copies, waits for them, and re-layouts: 31.3 us -> 4.53 us
    all_to_all x4 -> x0, starting transfers between devices: 25.6 us -> none  [the longest x1 7.58 us: body(): lax.all_to_all(grad_value_local[None], 'sp', split_axis=1, concat_axis=2,...]
    dot_general x22 -> x3, matrix products: 37.1 us -> 11.8 us  [the longest x1 7.06 us: dot_nt(): lax.dot_general(a, b, (((1,), (1,)), ((), ())), preferred_element_type=F32)]
    convert_element_type x11 -> x0, other arithmetic: 11.3 us -> none  [the longest x4 6.13 us: head_backward(): (softmaxes[:, 0] - lambda_col * softmaxes[:, 1]).astype(jnp.bfloat16)]
  transfers between devices with their start and end apart: 7 -> 1, of which waited for: 3 -> 0; matrix products, arithmetic and copies ran while one was open for 64% -> 5% of each run, Pallas kernels for 0% -> 79%
where the time goes in v1:
time: 171 us; the launch traced here: 169 us
  Pallas kernels  134 us (78%)
  between operations  14.1 us (8%)
  matrix products  11.8 us (7%)
  local copies, waits for them, and re-layouts  8.43 us (5%)
    pallas_call x1, Pallas kernels, gather(): pl.pallas_call(functools.partial(gather_kernel, n, m), out_shape=[jax.Sha...  102 us
    pallas_call x1, Pallas kernels, scatter(): pl.pallas_call(functools.partial(scatter_kernel, n, m), out_shape=[jax.Sh...  18.6 us
    pallas_call x1, Pallas kernels, attention(): pl.pallas_call(attention_kernel, grid=(heads,), in_specs=[pl.BlockSpec(me...  12.9 us
    dot_general x1, matrix products, dot_nt(): lax.dot_general(a, b, (((1,), (1,)), ((), ())), preferred_element_type=F32)  7.06 us
    unnamed x11, local copies, waits for them, and re-layouts  4.53 us
    dot_general x1, matrix products, body(): lax.dot_general(flat_tokens, grad_value, (((0,), (0,)), ((), ())), prefer...  3.52 us
  transfers between devices with their start and end apart: 1, of which 0 were waited for; matrix products, arithmetic and copies ran while one was open for 5% of the time, Pallas kernels for 79%

profile of v1, /device:TPU:0, one launch (start us, length us, event | category | flops | bytes accessed | tf_op | source)
XLA Modules:
  0.0 169.0 jit_solution(10795695624697418530)
XLA Ops:
  7.2 0.0 all-gather.2.cloned.1.call-start
  7.2 0.7 all-gather.2.cloned.1.call-update
  7.9 1.4 copy_bitcast_fusion.1
  9.3 0.0 copy-start
  9.3 0.9 copy-done
  10.2 0.0 copy-start.1
  10.2 1.0 copy-done.1
  11.3 0.0 copy-start.2
  11.3 1.0 copy-done.2
  12.3 102.4 %gather.1 = (bf16[8,128,2048]{2,1,0:T(8,128)(2,1)S(1)}, bf16[8,128,256]{2,1,0:T(8,128)(2,1)S(1)}, bf16[8,4,64,256]{3,2,1,0:T(8,128)(2,1)S(1)}) custom-call(bf16[128,2048]{1,0:T(8,128)(2,1)S(1)} %bitcast.26, bf16[128,2048]{1,0:T(8,128)(2,1)S(1)} %bitcast.27, bf16[64,2048]{1,0:T(8,128)(2,1)S(1)} %copy-done), custom_call_target="tpu_custom_call" | custom-call | flops 40000000000 | bytes 20000000 | tf_op jit(solution)/shard_map/gather/pallas_call | solution.py:275
  114.7 0.0 copy-start.4
  114.7 0.0 copy-start.3
  114.8 1.2 convolution_convert_fusion.2.v_ref
  116.0 0.7 copy-done.4
  116.7 0.0 copy-done.3
  116.7 12.9 %attention.1 = (bf16[1024,256]{1,0:T(8,128)(2,1)S(1)}, bf16[1024,256]{1,0:T(8,128)(2,1)S(1)}, bf16[1024,256]{1,0:T(8,128)(2,1)S(1)}, f32[2,8,128]{2,1,0:T(8,128)S(1)}) custom-call(f32[2]{0:T(128)S(1)} %copy-done.3, bf16[1024,256]{1,0:T(8,128)(2,1)S(1)} %get-tuple-element.26.q_ref, bf16[1024,256]{1,0:T(8,128)(2,1)S(1)} %get-tuple-element.25.k_ref, ...), custom_call_target="tpu_custom_call" | custom-call | flops 3221225472 | bytes 3670016 | tf_op jit(solution)/shard_map/attention/pallas_call | solution.py:110
  129.7 0.9 reshape.39
  130.6 0.9 reshape.40
  131.5 3.5 %convolution_convert_fusion = bf16[2048,256]{1,0:T(8,128)(2,1)S(1)} fusion(bf16[1024,2048]{1,0:T(8,128)(2,1)} %bitcast.29, bf16[1024,256]{1,0:T(8,128)(2,1)S(1)} %get-tuple-element.20.dv_ref), kind=kOutput, calls=%fused_computation | convolution fusion | flops 1074266112 | bytes 5767168 | tf_op jit(solution)/shard_map/dot_general | solution.py:425
  135.0 0.1 copy.17
  135.1 18.6 %scatter.1 = (bf16[128,2048]{1,0:T(8,128)(2,1)S(1)}, f32[64,2048]{1,0:T(8,128)S(1)}, f32[2,8,128]{2,1,0:T(8,128)S(1)}) custom-call(bf16[1024,256]{1,0:T(8,128)(2,1)S(1)} %get-tuple-element.20.dv_ref, bf16[4,8,64,256]{3,2,1,0:T(8,128)(2,1)S(1)} %bitcast.25, f32[2,8,128]{2,1,0:T(8,128)S(1)} %get-tuple-element.21.gl_ref), custom_call_target="tpu_custom_call" | custom-call | tf_op jit(solution)/shard_map/scatter/pallas_call | solution.py:374
  153.7 0.6 slice_reduce_fusion
  154.3 7.1 %fusion = bf16[1,128,2048]{2,1,0:T(8,128)(2,1)} fusion(bf16[128,2048]{1,0:T(8,128)(2,1)S(1)} %get-tuple-element.22, bf16[2048,2048]{1,0:T(8,128)(2,1)} %all-gather.2.cloned.1.call-done), kind=kOutput, calls=%fused_computation.2 | convolution fusion | flops 1074003968 | bytes 9437184 | tf_op jit(solution)/shard_map/dot_general | solution.py:23
  161.4 0.8 copy.19
  (1 shorter events, 0.0 us)
Async XLA Ops:
  7.2 147.2 %all-gather.2.cloned.1.call-start = ((), (), s32[]{:S(2)}) async-start(), calls=%async_computation | async-start | bytes 8650752 | tf_op jit(solution)/shard_map/all_gather | solution.py:407
  9.3 1.0 copy-start
  10.2 1.0 copy-start.1
  11.3 1.0 copy-start.2
  114.7 2.0 %copy-start.4 = (bf16[8,128,2048]{2,1,0:T(8,128)(2,1)}, bf16[8,128,2048]{2,1,0:T(8,128)(2,1)S(1)}, u32[]{:S(2)}) copy-start(bf16[8,128,2048]{2,1,0:T(8,128)(2,1)S(1)} %get-tuple-element.15) | copy-start | bytes 12582916
  114.7 2.0 %copy-start.3 = (f32[2]{0:T(128)S(1)}, f32[2]{0:T(128)}, u32[]{:S(2)}) copy-start(f32[2]{0:T(128)} %lam_ref.1) | copy-start | bytes 28
Sparse Core Ops, SparseCore 0:
  10.8 102.5 all-gather.1

commit v2 on v1

--- a/solution.py
+++ b/solution.py
@@ -303,21 +303,50 @@
 
 
 def scatter_kernel(
-    n, m, dv_ref, t_ref, gl_ref, dvt_ref, gw_ref, glo_ref, rbuf, sbuf, fbuf, lbuf,
-    local_sem, v_send, v_recv, t_send, t_recv, l_send, l_recv, f_send, f_recv,
+    n, m, part_ref, t_ref, gl_ref, gt_ref, gw_ref, glo_ref, rbuf, sbuf, fbuf, lbuf, rs_recv, rs_send,
+    local_sem, ring_send, ring_recv, t_send, t_recv, l_send, l_recv, f_send, f_recv,
 ):
     me = lax.axis_index("sp")
     my_dp = lax.axis_index("dp")
-    rows = dvt_ref.shape[0]
-    feats = dv_ref.shape[1]
+    rows = gt_ref.shape[0]
+    feats = t_ref.shape[3]
+    part = rows // (2 * CHUNKS)
+    place = ring_place(me, n)
+    sides = [
+        ring_member((place + 1) % n, n),
+        ring_member((place + n - 1) % n, n),
+    ]
     sp_peers = [(me + k) % n for k in range(1, n)]
     dp_peers = [(my_dp + k) % m for k in range(1, m)]
     greet([(s, my_dp) for s in sp_peers] + [(me, d) for d in dp_peers])
 
-    def tokens_of(s):
-        return dv_ref.at[pl.ds(pl.multiple_of(s * rows, rows), rows)]
-
-    mine = dvt_ref.at[:, pl.ds(pl.multiple_of(me * feats, feats), feats)]
+    def span(side, chunk):
+        return pl.ds((side * CHUNKS + chunk) * part, part)
+
+    def own_rows(step, side, chunk):
+        goal = (place + 2 * n - 1 - step) % n if side == 0 else (place + 1 + step) % n
+        start = ring_member(goal, n) * rows + (side * CHUNKS + chunk) * part
+        return pl.ds(pl.multiple_of(start, part), part)
+
+    def ring(step, side, chunk):
+        if step == 0:
+            src = part_ref.at[own_rows(0, side, chunk)]
+        else:
+            src = rs_send.at[step - 1, span(side, chunk)]
+        return remote(
+            src,
+            rs_recv.at[step, span(side, chunk)],
+            ring_send.at[step, side, chunk],
+            ring_recv.at[step, side, chunk],
+            sides[side],
+            my_dp,
+        )
+
+    order = [(side, chunk) for chunk in range(CHUNKS) for side in range(2)]
+    hops = {}
+    for side, chunk in order:
+        hops[0, side, chunk] = ring(0, side, chunk)
+        hops[0, side, chunk].start()
     t_copies = [
         remote(t_ref.at[d], rbuf.at[k], t_send.at[k], t_recv.at[k], me, d)
         for k, d in enumerate(dp_peers)
@@ -326,28 +355,34 @@
         remote(gl_ref, lbuf.at[k], l_send.at[k], l_recv.at[k], me, d)
         for k, d in enumerate(dp_peers)
     ]
-    v_copies = [
-        remote(tokens_of(s), mine, v_send.at[k], v_recv.at[k], s, my_dp)
-        for k, s in enumerate(sp_peers)
-    ]
-    for copy in l_copies + t_copies + v_copies:
+    for copy in l_copies + t_copies:
         copy.start()
-    own = pltpu.make_async_copy(tokens_of(me), mine, local_sem.at[0])
-    own.start()
-    for copy in t_copies:
-        copy.wait_recv()
-    total = t_ref[my_dp].astype(F32)
-    for k in range(m - 1):
-        total = total + rbuf[k].astype(F32)
-    sbuf[...] = total.astype(BF16)
     f_copies = [
         remote(sbuf.at[s], fbuf.at[me], f_send.at[k], f_recv.at[k], s, my_dp)
         for k, s in enumerate(sp_peers)
     ]
-    for copy in f_copies:
-        copy.start()
-    own_f = pltpu.make_async_copy(sbuf.at[me], fbuf.at[me], local_sem.at[1])
-    own_f.start()
+    own_f = pltpu.make_async_copy(sbuf.at[me], fbuf.at[me], local_sem.at[0])
+    for step in range(1, n):
+        for side, chunk in order:
+            hops[step - 1, side, chunk].wait_recv()
+            total = rs_recv[step - 1, span(side, chunk)].astype(F32)
+            total = total + part_ref[own_rows(step, side, chunk)].astype(F32)
+            if step < n - 1:
+                rs_send[step - 1, span(side, chunk)] = total.astype(BF16)
+                hops[step, side, chunk] = ring(step, side, chunk)
+                hops[step, side, chunk].start()
+            else:
+                gt_ref[span(side, chunk)] = total.astype(BF16)
+        if step == n // 2 - 1:
+            for copy in t_copies:
+                copy.wait_recv()
+            term = t_ref[my_dp].astype(F32)
+            for k in range(m - 1):
+                term = term + rbuf[k].astype(F32)
+            sbuf[...] = term.astype(BF16)
+            for copy in f_copies:
+                copy.start()
+            own_f.start()
     for copy in l_copies:
         copy.wait_recv()
     lam = gl_ref[...]
@@ -359,22 +394,20 @@
         copy.wait_recv()
     for s in range(n):
         gw_ref[:, s * feats : (s + 1) * feats] = fbuf[s].astype(F32)
-    own.wait()
-    for copy in v_copies:
-        copy.wait_recv()
-    for copy in l_copies + t_copies + v_copies + f_copies:
+    for copy in list(hops.values()) + l_copies + t_copies + f_copies:
         copy.wait_send()
 
 
-def scatter(grad_value, term, grad_lambda, n, m):
-    length, feats = grad_value.shape
-    row_count = term.shape[2]
+def scatter(partial, term, grad_lambda, n, m):
+    length, depth = partial.shape
+    row_count, feats = term.shape[2:]
+    rows = length // n
     vmem = pl.BlockSpec(memory_space=pltpu.VMEM)
     dma = pltpu.SemaphoreType.DMA
     return pl.pallas_call(
         functools.partial(scatter_kernel, n, m),
         out_shape=[
-            jax.ShapeDtypeStruct((length // n, n * feats), BF16),
+            jax.ShapeDtypeStruct((rows, depth), BF16),
             jax.ShapeDtypeStruct((row_count, n * feats), F32),
             jax.ShapeDtypeStruct(grad_lambda.shape, F32),
         ],
@@ -385,9 +418,11 @@
             pltpu.VMEM(term.shape[1:], BF16),
             pltpu.VMEM(term.shape[1:], BF16),
             pltpu.VMEM((m - 1,) + grad_lambda.shape, F32),
-            dma((2,)),
-            dma((n - 1,)),
-            dma((n - 1,)),
+            pltpu.VMEM((n - 1, rows, depth), BF16),
+            pltpu.VMEM((max(n - 2, 1), rows, depth), BF16),
+            dma((1,)),
+            dma((n - 1, 2, CHUNKS)),
+            dma((n - 1, 2, CHUNKS)),
             dma((m - 1,)),
             dma((m - 1,)),
             dma((m - 1,)),
@@ -396,24 +431,22 @@
             dma((n - 1,)),
         ],
         compiler_params=pltpu.CompilerParams(
-            collective_id=1, has_side_effects=True, vmem_limit_bytes=40 * 1024 * 1024
+            collective_id=1, has_side_effects=True, vmem_limit_bytes=48 * 1024 * 1024
         ),
         name="scatter",
-    )(grad_value, term, grad_lambda)
+    )(partial, term, grad_lambda)
 
 
 def body(n, m, tokens, cotangent, value_weight, query_heads, key_heads, lambdas):
     row_count, feature_count = value_weight.shape
-    all_weight = lax.all_gather(value_weight, ("sp", "dp"), axis=0, tiled=True)
     all_tokens, cotan_heads, weight_cols = gather(tokens[0], cotangent[0], value_weight, n, m)
     feats = feature_count // n
     depth = n * m * row_count
     length = all_tokens.shape[0] * all_tokens.shape[1]
     head_count, width = query_heads.shape[2], query_heads.shape[3]
     flat_tokens = all_tokens.reshape(length, depth)
-    values = jnp.dot(
-        flat_tokens, weight_cols.reshape(depth, feats), preferred_element_type=F32
-    ).astype(BF16)
+    weight_cols = weight_cols.reshape(depth, feats)
+    values = jnp.dot(flat_tokens, weight_cols, preferred_element_type=F32).astype(BF16)
     grad_query, grad_key, grad_value, grad_lambda = attention(
         lambdas,
         query_heads.reshape(length, feats),
@@ -426,12 +459,12 @@
         flat_tokens, grad_value, (((0,), (0,)), ((), ())), preferred_element_type=F32
     ).astype(BF16)
     term = term.reshape(n, m, row_count, feats).transpose(1, 0, 2, 3)
-    grad_value_tokens, grad_weight, lambda_sum = scatter(grad_value, term, grad_lambda, n, m)
-    grad_tokens = dot_nt(grad_value_tokens, all_weight).astype(BF16)[None]
+    partial = dot_nt(grad_value, weight_cols).astype(BF16)
+    grad_tokens, grad_weight, lambda_sum = scatter(partial, term, grad_lambda, n, m)
     return (
         grad_query.reshape(1, length, head_count, width),
         grad_key.reshape(1, length, head_count, width),
-        grad_tokens,
+        grad_tokens[None],
         grad_weight,
         lambda_sum[:, 0, 0],
     )

time: 171 us -> 144 us (0.84)
  between operations: 14.1 us -> 0.72 us
  Pallas kernels: 134 us -> 128 us
  matrix products: 11.8 us -> 5.81 us
    pallas_call x1, Pallas kernels: 102 us -> 63.3 us  [gather(): pl.pallas_call(functools.partial(gather_kernel, n, m), out_shape=[jax.Sha...]
    pallas_call x1, Pallas kernels: 18.6 us -> 51.3 us  [scatter(): pl.pallas_call(functools.partial(scatter_kernel, n, m), out_shape=[jax.Sh...]
    dot_general x1, matrix products: 7.06 us -> 3.23 us  [dot_nt(): lax.dot_general(a, b, (((1,), (1,)), ((), ())), preferred_element_type=F32)]
    dot_general x1, matrix products: 3.52 us -> 1.33 us  [body(): lax.dot_general(flat_tokens, grad_value, (((0,), (0,)), ((), ())), prefer...]
    unnamed x11 -> x12, local copies, waits for them, and re-layouts: 4.53 us -> 4.63 us
  transfers between devices with their start and end apart: 1 -> 0, of which waited for: 0 -> 0; matrix products, arithmetic and copies ran while one was open for 5% -> 0% of each run, Pallas kernels for 79% -> 0%
where the time goes in v2:
time: 144 us
  Pallas kernels  128 us (89%)
  local copies, waits for them, and re-layouts  9.54 us (7%)
  matrix products  5.81 us (4%)
    pallas_call x1, Pallas kernels, gather(): pl.pallas_call(functools.partial(gather_kernel, n, m), out_shape=[jax.Sha...  63.3 us
    pallas_call x1, Pallas kernels, scatter(): pl.pallas_call(functools.partial(scatter_kernel, n, m), out_shape=[jax.Sh...  51.3 us
    pallas_call x1, Pallas kernels, attention(): pl.pallas_call(attention_kernel, grid=(heads,), in_specs=[pl.BlockSpec(me...  13 us
    unnamed x12, local copies, waits for them, and re-layouts  4.63 us
    dot_general x1, matrix products, dot_nt(): lax.dot_general(a, b, (((1,), (1,)), ((), ())), preferred_element_type=F32)  3.23 us

profile of v2, /device:TPU:0, one launch (start us, length us, event | category | flops | bytes accessed | tf_op | source)
XLA Modules:
  0.0 143.6 jit_solution(13147543404560112047)
XLA Ops:
  0.6 1.4 copy_bitcast_fusion.1
  2.0 0.0 copy-start.1
  2.0 1.0 copy-done.1
  3.0 0.0 copy-start.2
  3.0 1.0 copy-done.2
  4.1 0.0 copy-start.3
  4.1 0.9 copy-done.3
  5.0 63.3 %gather.1 = (bf16[8,128,2048]{2,1,0:T(8,128)(2,1)S(1)}, bf16[8,128,256]{2,1,0:T(8,128)(2,1)S(1)}, bf16[8,4,64,256]{3,2,1,0:T(8,128)(2,1)S(1)}) custom-call(bf16[128,2048]{1,0:T(8,128)(2,1)S(1)} %bitcast.28, bf16[128,2048]{1,0:T(8,128)(2,1)S(1)} %bitcast.29, bf16[64,2048]{1,0:T(8,128)(2,1)S(1)} %copy-done.3), custom_call_target="tpu_custom_call" | custom-call | flops 40000000000 | bytes 20000000 | tf_op jit(solution)/shard_map/gather/pallas_call | solution.py:275
  68.3 0.0 copy-start.4
  68.4 1.2 convolution_convert_fusion.2.v_ref
  69.6 0.0 copy-done.4
  69.6 13.0 %attention.1 = (bf16[1024,256]{1,0:T(8,128)(2,1)S(1)}, bf16[1024,256]{1,0:T(8,128)(2,1)S(1)}, bf16[1024,256]{1,0:T(8,128)(2,1)S(1)}, f32[2,8,128]{2,1,0:T(8,128)S(1)}) custom-call(f32[2]{0:T(128)S(1)} %copy-done.4, bf16[1024,256]{1,0:T(8,128)(2,1)S(1)} %get-tuple-element.26.q_ref, bf16[1024,256]{1,0:T(8,128)(2,1)S(1)} %get-tuple-element.25.k_ref, ...), custom_call_target="tpu_custom_call" | custom-call | flops 3221225472 | bytes 3670016 | tf_op jit(solution)/shard_map/attention/pallas_call | solution.py:110
  82.6 0.0 copy-start
  82.6 1.3 convolution_convert_fusion.1
  83.9 0.0 copy-done
  84.0 0.1 copy.17
  84.0 2.0 %reshape.39 = bf16[1,1024,2,128]{3,2,1,0:T(2,128)(2,1)} reshape(bf16[1024,256]{1,0:T(8,128)(2,1)} %copy-done) | data formatting | bytes 1048576 | tf_op jit(solution)/shard_map/reshape | solution.py:465
  86.0 0.9 reshape.40
  86.9 3.2 %convolution_convert_fusion.part_ref = bf16[1024,2048]{1,0:T(8,128)(2,1)} fusion(bf16[1024,256]{1,0:T(8,128)(2,1)S(1)} %get-tuple-element.20, bf16[2048,256]{1,0:T(8,128)(2,1)S(1)} %bitcast.26), kind=kOutput, calls=%fused_computation | convolution fusion | flops 1075838976 | bytes 5767168 | tf_op jit(solution)/shard_map/dot_general | solution.py:23
  90.1 51.3 %scatter.1 = (bf16[128,2048]{1,0:T(8,128)(2,1)S(1)}, f32[64,2048]{1,0:T(8,128)S(1)}, f32[2,8,128]{2,1,0:T(8,128)S(1)}) custom-call(bf16[1024,2048]{1,0:T(8,128)(2,1)} %convolution_convert_fusion.part_ref, bf16[4,8,64,256]{3,2,1,0:T(8,128)(2,1)S(1)} %bitcast.24, f32[2,8,128]{2,1,0:T(8,128)S(1)} %get-tuple-element.21.gl_ref), custom_call_target="tpu_custom_call" | custom-call | tf_op jit(solution)/shard_map/scatter/pallas_call | solution.py:407
  141.4 0.6 slice_reduce_fusion
  142.0 0.8 copy.20
  142.8 0.8 copy.21
Async XLA Ops:
  2.0 1.0 copy-start.1
  3.0 1.0 copy-start.2
  4.1 0.9 copy-start.3
  68.3 1.3 copy-start.4
  82.6 1.4 copy-start

commit v3 on v2

--- a/solution.py
+++ b/solution.py
@@ -10,7 +10,7 @@
 QBLOCK = 256
 EPS = 1e-06
 NEGATIVE = -1e30
-CHUNKS = 2
+CHUNKS = 4
 F32 = jnp.float32
 BF16 = jnp.bfloat16
 
@@ -279,7 +279,7 @@
             jax.ShapeDtypeStruct((n, rows, feats), BF16),
             jax.ShapeDtypeStruct((n, m, weight.shape[0], feats), BF16),
         ],
-        in_specs=[vmem] * 3,
+        in_specs=[pl.BlockSpec(memory_space=pl.ANY)] * 3,
         out_specs=[vmem] * 3,
         scratch_shapes=[
             dma((3,)),
@@ -293,7 +293,7 @@
             dma((m // 2,)),
         ],
         compiler_params=pltpu.CompilerParams(
-            collective_id=0, has_side_effects=True, vmem_limit_bytes=40 * 1024 * 1024
+            collective_id=0, has_side_effects=True, vmem_limit_bytes=60 * 1024 * 1024
         ),
         cost_estimate=pl.CostEstimate(
             flops=40_000_000_000, bytes_accessed=20_000_000, transcendentals=0

time: 144 us -> 147 us (1.021)
  local copies, waits for them, and re-layouts: 9.54 us -> 5.47 us
  matrix products: 5.81 us -> 9.59 us
  Pallas kernels: 128 us -> 131 us
    unnamed x12 -> x8, local copies, waits for them, and re-layouts: 4.63 us -> 1.6 us
    dot_general x1, matrix products: 1.25 us -> 3.79 us  [body(): jnp.dot(flat_tokens, weight_cols, preferred_element_type=F32).astype(BF16)]
    pallas_call x1, Pallas kernels: 51.3 us -> 52.9 us  [scatter(): pl.pallas_call(functools.partial(scatter_kernel, n, m), out_shape=[jax.Sh...]
where the time goes in v3:
time: 147 us; the launch traced here: 146 us
  Pallas kernels  131 us (89%)
  matrix products  9.59 us (7%)
  local copies, waits for them, and re-layouts  5.47 us (4%)
    pallas_call x1, Pallas kernels, gather(): pl.pallas_call(functools.partial(gather_kernel, n, m), out_shape=[jax.Sha...  64.7 us
    pallas_call x1, Pallas kernels, scatter(): pl.pallas_call(functools.partial(scatter_kernel, n, m), out_shape=[jax.Sh...  52.9 us
    pallas_call x1, Pallas kernels, attention(): pl.pallas_call(attention_kernel, grid=(heads,), in_specs=[pl.BlockSpec(me...  13 us
    dot_general x1, matrix products, dot_nt(): lax.dot_general(a, b, (((1,), (1,)), ((), ())), preferred_element_type=F32)  4.45 us
    dot_general x1, matrix products, body(): jnp.dot(flat_tokens, weight_cols, preferred_element_type=F32).astype(BF16)  3.79 us

profile of v3, /device:TPU:0, one launch (start us, length us, event | category | flops | bytes accessed | tf_op | source)
XLA Modules:
  0.0 146.4 jit_solution(9748842713815733557)
XLA Ops:
  0.6 1.4 copy_bitcast_fusion.1
  2.0 64.7 %gather.1 = (bf16[8,128,2048]{2,1,0:T(8,128)(2,1)}, bf16[8,128,256]{2,1,0:T(8,128)(2,1)}, bf16[8,4,64,256]{3,2,1,0:T(8,128)(2,1)}) custom-call(bf16[128,2048]{1,0:T(8,128)(2,1)} %bitcast.32, bf16[128,2048]{1,0:T(8,128)(2,1)} %bitcast.33, bf16[64,2048]{1,0:T(8,128)(2,1)} %w_ref.1), custom_call_target="tpu_custom_call" | custom-call | flops 40000000000 | bytes 20000000 | tf_op jit(solution)/shard_map/gather/pallas_call | solution.py:275
  66.7 0.0 copy-start
  66.7 0.0 copy-start.1
  66.8 3.8 %convolution_convert_fusion.2.v_ref = bf16[1024,256]{1,0:T(8,128)(2,1)S(1)} fusion(bf16[1024,2048]{1,0:T(8,128)(2,1)} %bitcast.34, bf16[2048,256]{1,0:T(8,128)(2,1)} %bitcast.27), kind=kOutput, calls=%fused_computation.2 | convolution fusion | flops 1074003968 | bytes 5767168 | tf_op jit(solution)/shard_map/dot_general | solution.py:449
  70.5 0.0 copy-done
  70.6 0.0 copy-done.1
  70.6 0.0 copy-start.2
  70.6 13.0 %attention.1 = (bf16[1024,256]{1,0:T(8,128)(2,1)S(1)}, bf16[1024,256]{1,0:T(8,128)(2,1)S(1)}, bf16[1024,256]{1,0:T(8,128)(2,1)S(1)}, f32[2,8,128]{2,1,0:T(8,128)S(1)}) custom-call(f32[2]{0:T(128)S(1)} %copy-done, bf16[1024,256]{1,0:T(8,128)(2,1)S(1)} %get-tuple-element.26.q_ref, bf16[1024,256]{1,0:T(8,128)(2,1)S(1)} %get-tuple-element.25.k_ref, ...), custom_call_target="tpu_custom_call" | custom-call | flops 3221225472 | bytes 3670016 | tf_op jit(solution)/shard_map/attention/pallas_call | solution.py:110
  83.5 0.0 copy-done.2
  83.6 1.3 convolution_convert_fusion.1
  84.9 0.1 copy.17
  85.0 0.9 reshape.39
  85.9 0.9 reshape.40
  86.8 4.5 %convolution_convert_fusion.part_ref = bf16[1024,2048]{1,0:T(8,128)(2,1)} fusion(bf16[1024,256]{1,0:T(8,128)(2,1)S(1)} %get-tuple-element.20, bf16[2048,256]{1,0:T(8,128)(2,1)} %bitcast.28), kind=kOutput, calls=%fused_computation | convolution fusion | flops 1075838976 | bytes 5767168 | tf_op jit(solution)/shard_map/dot_general | solution.py:23
  91.3 52.9 %scatter.1 = (bf16[128,2048]{1,0:T(8,128)(2,1)S(1)}, f32[64,2048]{1,0:T(8,128)S(1)}, f32[2,8,128]{2,1,0:T(8,128)S(1)}) custom-call(bf16[1024,2048]{1,0:T(8,128)(2,1)} %convolution_convert_fusion.part_ref, bf16[4,8,64,256]{3,2,1,0:T(8,128)(2,1)S(1)} %bitcast.24, f32[2,8,128]{2,1,0:T(8,128)S(1)} %get-tuple-element.21.gl_ref), custom_call_target="tpu_custom_call" | custom-call | tf_op jit(solution)/shard_map/scatter/pallas_call | solution.py:407
  144.2 0.6 slice_reduce_fusion
  144.8 0.8 copy.20
  145.6 0.8 copy.21
Async XLA Ops:
  66.7 3.8 %copy-start = (f32[2]{0:T(128)S(1)}, f32[2]{0:T(128)}, u32[]{:S(2)}) copy-start(f32[2]{0:T(128)} %lam_ref.1) | copy-start | bytes 28
  66.7 3.8 %copy-start.1 = (bf16[8,128,256]{2,1,0:T(8,128)(2,1)S(1)}, bf16[8,128,256]{2,1,0:T(8,128)(2,1)}, u32[]{:S(2)}) copy-start(bf16[8,128,256]{2,1,0:T(8,128)(2,1)} %get-tuple-element.17) | copy-start | bytes 1572868
  70.6 13.0 %copy-start.2 = (bf16[8,128,2048]{2,1,0:T(8,128)(2,1)S(1)}, bf16[8,128,2048]{2,1,0:T(8,128)(2,1)}, u32[]{:S(2)}) copy-start(bf16[8,128,2048]{2,1,0:T(8,128)(2,1)} %get-tuple-element.15) | copy-start | bytes 12582916
